TPU v7x, 32 devices: a whole 2x2x4 slice. The times are simulated.
32 devices in a mesh: sp: 8 (over z, x), tp: 4 (over y, core).
Axes of the slice: x: 2, y: 2, z: 4, core: 2. Of those that a mesh axis runs over, the one named last changes fastest.
Arguments:
- tokens: bfloat16 [2, 128, 1024], P(None, 'sp', 'tp'), may hold values from -6 to 6
- in_weight: bfloat16 [3, 1024, 2048], P(None, 'sp', 'tp'), may hold values from -0.1875 to 0.1875
- gate_weight: bfloat16 [3, 1024, 2048], P(None, 'sp', 'tp'), may hold values from -0.1875 to 0.1875
- out_weight: bfloat16 [3, 2048, 1024], P(None, 'tp', 'sp'), may hold values from -0.25 to 0.25
- recur_weight: bfloat16 [3, 2, 16, 128, 128], P(None, None, 'tp'), may hold values from -0.5 to 0.5
- input_weight: bfloat16 [3, 2, 16, 128, 128], P(None, None, 'tp'), may hold values from -0.5 to 0.5
- conv_taps: bfloat16 [3, 4, 2048], P(None, None, 'tp'), may hold values from -3 to 3
- decay_rate: float32 [3, 2, 2048], P(None, None, 'tp'), may hold values from 0.02 to 0.25
- norm_gain: float32 [3, 1024], replicated, may hold values from 0.5 to 1.5
Outputs:
- mixed_out: bfloat16 [2, 128, 1024], P(None, 'sp', 'tp')
All inputs are finite; a program needn't handle non-finite values.
Results may differ from a plain program's by a relative error of at most 0.04.
Values may be sent and summed in bfloat16 or wider, within the bound.
A program may use at most 64 MiB of HBM per device.

v0:
```python
import jax
import jax.numpy as jnp
from jax import lax
from jax.sharding import PartitionSpec as P

LAYERS = 3
epsilon = 1e-06
gate_power = 8.0


def extended(array, sides, width, wrap):
    for axis, dim in sides:
        size, length = (lax.axis_size(axis), array.shape[dim])
        up = [(i, (i + 1) % size) for i in range(size if wrap else size - 1)]
        down = [(j, i) for i, j in up]
        last = lax.slice_in_dim(array, length - width, length, axis=dim)
        initial = lax.slice_in_dim(array, 0, width, axis=dim)
        before = lax.ppermute(last, axis, up)
        after = lax.ppermute(initial, axis, down)
        array = jnp.concatenate([before, array, after], axis=dim)
    return array


def carried_in(value, axis, join, neutral, backward):
    count, mine = (lax.axis_size(axis), lax.axis_index(axis))
    pieces = jax.tree.map(lambda part: lax.all_gather(part, axis), value)
    if backward:
        pieces = jax.tree.map(lambda part: part[::-1], pieces)
        mine = count - 1 - mine
    subtotal = jax.tree.map(
        lambda part, zero: jnp.full_like(part, 0) + jnp.asarray(zero, part.dtype), value, neutral
    )

    def hop(position, subtotal):
        longer = join(subtotal, jax.tree.map(lambda part: part[position], pieces))
        return jax.tree.map(lambda new, old: jnp.where(position < mine, new, old), longer, subtotal)

    return lax.fori_loop(0, count - 1, hop, subtotal)


def combine(earlier, later_pair):
    first_decay, first_drive = earlier
    second_decay, second_drive = later_pair
    return (first_decay * second_decay, second_decay * first_drive + second_drive)


def body(
    tokens,
    in_weight,
    gate_weight,
    out_weight,
    recur_weight,
    input_weight,
    conv_taps,
    decay_rate,
    norm_gain,
):
    batch_size, tok_rows, _ = tokens.shape
    seq_len = tok_rows * lax.axis_size("sp")
    chan_width = in_weight.shape[2]
    in_whole, gate_whole = (
        lax.all_gather(in_weight, "sp", axis=1, tiled=True),
        lax.all_gather(gate_weight, "sp", axis=1, tiled=True),
    )
    out_whole = lax.all_gather(out_weight, "sp", axis=2, tiled=True)
    state = tokens
    for layer_index in range(LAYERS):
        gathered = lax.all_gather(state, "tp", axis=2, tiled=True)
        flat_rows = gathered.reshape(batch_size * tok_rows, -1).astype(jnp.float32)
        scale_rows = lax.rsqrt(jnp.mean(flat_rows * flat_rows, axis=-1, keepdims=True) + epsilon)
        normed = (flat_rows * scale_rows * norm_gain[layer_index]).astype(jnp.bfloat16)
        branch = jnp.dot(normed, in_whole[layer_index], preferred_element_type=jnp.float32)
        gate_branch = jnp.dot(normed, gate_whole[layer_index], preferred_element_type=jnp.float32)
        branch = branch.astype(jnp.bfloat16).reshape(batch_size, tok_rows, chan_width)
        gate_branch = gate_branch.astype(jnp.bfloat16).reshape(batch_size, tok_rows, chan_width)
        padded = extended(branch, (("sp", 1),), 2, False)
        tap_values = conv_taps[layer_index].astype(jnp.float32)
        conv_out = padded[:, 0:tok_rows].astype(jnp.float32) * tap_values[0]
        for tap_index in range(1, tap_values.shape[0]):
            conv_out = (
                conv_out
                + padded[:, tap_index : tap_index + tok_rows].astype(jnp.float32)
                * tap_values[tap_index]
            )
        conv_out = conv_out.astype(jnp.bfloat16)
        conv_float = conv_out.astype(jnp.float32)
        recur_full = recur_weight[layer_index]
        input_full = input_weight[layer_index]
        heads_local = recur_full.shape[1]
        head_dim = recur_full.shape[2]
        blocks = conv_out.reshape(batch_size, tok_rows, heads_local, head_dim)
        hidden_sum = jnp.zeros((batch_size, tok_rows, chan_width), jnp.float32)
        identity = (
            jnp.ones((batch_size, chan_width), jnp.float32),
            jnp.zeros((batch_size, chan_width), jnp.float32),
        )
        for direction in range(2):
            recur_gate = jax.nn.sigmoid(
                jnp.einsum(
                    "bthd,hde->bthe",
                    blocks,
                    recur_full[direction],
                    preferred_element_type=jnp.float32,
                )
            ).reshape(batch_size, tok_rows, chan_width)
            input_gate = jax.nn.sigmoid(
                jnp.einsum(
                    "bthd,hde->bthe",
                    blocks,
                    input_full[direction],
                    preferred_element_type=jnp.float32,
                )
            ).reshape(batch_size, tok_rows, chan_width)
            log_decay = -gate_power * recur_gate * decay_rate[layer_index, direction] / seq_len
            decay_step = jnp.exp(log_decay)
            driven = jnp.sqrt(-jnp.expm1(2.0 * log_decay)) * input_gate * conv_float
            backward = direction == 1
            cum_decay, cum_drive = lax.associative_scan(
                combine, (decay_step, driven), axis=1, reverse=backward
            )
            if backward:
                totals = (cum_decay[:, 0], cum_drive[:, 0])
                incoming = carried_in(totals, "sp", combine, identity, True)
            else:
                totals = (cum_decay[:, -1], cum_drive[:, -1])
                incoming = carried_in(totals, "sp", combine, identity, False)
            hidden_sum = hidden_sum + (cum_decay * incoming[1][:, None, :] + cum_drive)
        mixed_rows = (hidden_sum * jax.nn.silu(gate_branch.astype(jnp.float32))).astype(
            jnp.bfloat16
        )
        mixed_rows = mixed_rows.reshape(batch_size * tok_rows, chan_width)
        partial_terms = jnp.dot(
            mixed_rows, out_whole[layer_index], preferred_element_type=jnp.float32
        )
        shard_sum = lax.psum_scatter(
            partial_terms.astype(jnp.bfloat16), "tp", scatter_dimension=1, tiled=True
        ).astype(jnp.float32)
        state = shard_sum.astype(jnp.bfloat16).reshape(batch_size, tok_rows, -1)
    return state


def solution(mesh):
    in_specs = (
        P(None, "sp", "tp"),
        P(None, "sp", "tp"),
        P(None, "sp", "tp"),
        P(None, "tp", "sp"),
        P(None, None, "tp", None, None),
        P(None, None, "tp", None, None),
        P(None, None, "tp"),
        P(None, None, "tp"),
        P(),
    )
    out_specs = P(None, "sp", "tp")
    return jax.shard_map(body, mesh=mesh, in_specs=in_specs, out_specs=out_specs, check_vma=False)
```

profile of v0, /device:TPU:0, one launch (start us, length us, event | category | flops | bytes accessed | tf_op | source)
XLA Modules:
  0.0 657.9 jit_solution(7241306334868398253)
XLA Ops:
  12.4 6.5 all_gather.54
  19.1 53.2 %all-gather.16.cloned.1.call-done = bf16[3,1024,512]{2,1,0:T(8,128)(2,1)} async-done(((bf16[3,128,512]{2,1,0:T(8,128)(2,1)}), bf16[3,1024,512]{2,1,0:T(8,128)(2,1)}) %all-gather.16.cloned.1.call-update) | async-done | bytes 3145744 | tf_op jit(solution)/shard_map/all_gather | solution.py:62
  72.3 1.5 convolution_convert_fusion.8
  75.1 4.5 collective-permute-start
  79.7 53.5 %all-gather.18.cloned.1.call-done = bf16[3,1024,512]{2,1,0:T(8,128)(2,1)} async-done(((bf16[3,128,512]{2,1,0:T(8,128)(2,1)}), bf16[3,1024,512]{2,1,0:T(8,128)(2,1)}) %all-gather.18.cloned.1.call-update) | async-done | bytes 3145744 | tf_op jit(solution)/shard_map/all_gather | solution.py:63
  133.2 1.5 convolution_convert_fusion.7
  138.2 30.9 %all-gather.2 = f32[16,1,512]{2,1,0:T(1,128)S(1)} all-gather(f32[2,1,512]{2,1,0:T(1,128)S(1)} %slice_add_fusion.19), channel_id=4, replica_groups=mesh['sp'=8,'tp'=4] {'sp'}, dimensions={0}, use_global_device_ids=true | all-gather | bytes 36864 | tf_op jit(solution)/shard_map/all_gather | solution.py:26
  169.2 31.4 %all-gather.3 = f32[16,1,512]{2,1,0:T(1,128)S(1)} all-gather(f32[2,1,512]{2,1,0:T(1,128)S(1)} %slice_add_fusion.16), channel_id=5, replica_groups=mesh['sp'=8,'tp'=4] {'sp'}, dimensions={0}, use_global_device_ids=true | all-gather | bytes 36864 | tf_op jit(solution)/shard_map/all_gather | solution.py:26
  201.5 30.6 %all-gather = f32[16,1,512]{2,1,0:T(1,128)S(1)} all-gather(f32[2,1,512]{2,1,0:T(1,128)S(1)} %slice_add_fusion.23), channel_id=2, replica_groups=mesh['sp'=8,'tp'=4] {'sp'}, dimensions={0}, use_global_device_ids=true | all-gather | bytes 36864 | tf_op jit(solution)/shard_map/all_gather | solution.py:26
  232.2 30.6 %all-gather.1 = f32[16,1,512]{2,1,0:T(1,128)S(1)} all-gather(f32[2,1,512]{2,1,0:T(1,128)S(1)} %slice_add_fusion.20), channel_id=3, replica_groups=mesh['sp'=8,'tp'=4] {'sp'}, dimensions={0}, use_global_device_ids=true | all-gather | bytes 36864 | tf_op jit(solution)/shard_map/all_gather | solution.py:26
  263.6 2.1 convolution_convert_fusion.2
  266.4 17.8 %reduce-scatter.4.cloned.1.call-done = bf16[32,256]{1,0:T(8,128)(2,1)} async-done(((bf16[32,1024]{1,0:T(8,128)(2,1)}), bf16[32,256]{1,0:T(8,128)(2,1)}) %reduce-scatter.4.cloned.1.call-update) | async-done | bytes 16400 | tf_op jit(solution)/shard_map/reduce_scatter | solution.py:135
  284.2 5.4 all_gather.62
  289.9 1.5 convolution_convert_fusion.6
  292.7 4.5 collective-permute-start.2
  297.3 2.1 convolution_convert_fusion.5
  306.9 32.5 %all-gather.6 = f32[16,1,512]{2,1,0:T(1,128)S(1)} all-gather(f32[2,1,512]{2,1,0:T(1,128)S(1)} %slice_add_fusion.11), channel_id=8, replica_groups=mesh['sp'=8,'tp'=4] {'sp'}, dimensions={0}, use_global_device_ids=true | all-gather | bytes 36864 | tf_op jit(solution)/shard_map/all_gather | solution.py:26
  339.6 30.6 %all-gather.7 = f32[16,1,512]{2,1,0:T(1,128)S(1)} all-gather(f32[2,1,512]{2,1,0:T(1,128)S(1)} %slice_add_fusion.8), channel_id=9, replica_groups=mesh['sp'=8,'tp'=4] {'sp'}, dimensions={0}, use_global_device_ids=true | all-gather | bytes 36864 | tf_op jit(solution)/shard_map/all_gather | solution.py:26
  374.0 30.6 %all-gather.4 = f32[16,1,512]{2,1,0:T(1,128)S(1)} all-gather(f32[2,1,512]{2,1,0:T(1,128)S(1)} %slice_add_fusion.15), channel_id=6, replica_groups=mesh['sp'=8,'tp'=4] {'sp'}, dimensions={0}, use_global_device_ids=true | all-gather | bytes 36864 | tf_op jit(solution)/shard_map/all_gather | solution.py:26
  406.0 32.0 %all-gather.5 = f32[16,1,512]{2,1,0:T(1,128)} all-gather(f32[2,1,512]{2,1,0:T(1,128)S(1)} %slice_add_fusion.12), channel_id=7, replica_groups=mesh['sp'=8,'tp'=4] {'sp'}, dimensions={0}, use_global_device_ids=true | all-gather | bytes 36864 | tf_op jit(solution)/shard_map/all_gather | solution.py:26
  440.9 5.0 while.86
  447.7 17.9 %reduce-scatter.6.cloned.1.call-done = bf16[32,256]{1,0:T(8,128)(2,1)} async-done(((bf16[32,1024]{1,0:T(8,128)(2,1)}), bf16[32,256]{1,0:T(8,128)(2,1)}) %reduce-scatter.6.cloned.1.call-update) | async-done | bytes 16400 | tf_op jit(solution)/shard_map/reduce_scatter | solution.py:135
  465.7 5.4 all_gather.67
  472.0 1.5 convolution_convert_fusion.4
  474.8 4.7 collective-permute-start.4
  479.6 2.1 convolution_convert_fusion.3
  492.6 32.3 %all-gather.10 = f32[16,1,512]{2,1,0:T(1,128)S(1)} all-gather(f32[2,1,512]{2,1,0:T(1,128)S(1)} %slice_add_fusion.3), channel_id=12, replica_groups=mesh['sp'=8,'tp'=4] {'sp'}, dimensions={0}, use_global_device_ids=true | all-gather | bytes 36864 | tf_op jit(solution)/shard_map/all_gather | solution.py:26
  525.1 30.6 %all-gather.11 = f32[16,1,512]{2,1,0:T(1,128)S(1)} all-gather(f32[2,1,512]{2,1,0:T(1,128)S(1)} %slice_add_fusion), channel_id=13, replica_groups=mesh['sp'=8,'tp'=4] {'sp'}, dimensions={0}, use_global_device_ids=true | all-gather | bytes 36864 | tf_op jit(solution)/shard_map/all_gather | solution.py:26
  559.4 30.6 %all-gather.8 = f32[16,1,512]{2,1,0:T(1,128)S(1)} all-gather(f32[2,1,512]{2,1,0:T(1,128)S(1)} %slice_add_fusion.7), channel_id=10, replica_groups=mesh['sp'=8,'tp'=4] {'sp'}, dimensions={0}, use_global_device_ids=true | all-gather | bytes 36864 | tf_op jit(solution)/shard_map/all_gather | solution.py:26
  591.5 32.2 %all-gather.9 = f32[16,1,512]{2,1,0:T(1,128)} all-gather(f32[2,1,512]{2,1,0:T(1,128)S(1)} %slice_add_fusion.4), channel_id=11, replica_groups=mesh['sp'=8,'tp'=4] {'sp'}, dimensions={0}, use_global_device_ids=true | all-gather | bytes 36864 | tf_op jit(solution)/shard_map/all_gather | solution.py:26
  626.6 5.0 while.88
  633.3 17.8 %reduce-scatter.8.cloned.1.call-done = bf16[32,256]{1,0:T(8,128)(2,1)} async-done(((bf16[32,1024]{1,0:T(8,128)(2,1)}), bf16[32,256]{1,0:T(8,128)(2,1)}) %reduce-scatter.8.cloned.1.call-update) | async-done | bytes 16400 | tf_op jit(solution)/shard_map/reduce_scatter | solution.py:135
  (504 shorter events, 63.9 us)
Async XLA Ops:
  6.5 128.2 %copy-start.3 = (bf16[3,2,4,128,128]{4,3,2,1,0:T(8,128)(2,1)S(1)}, bf16[3,2,4,128,128]{4,3,2,1,0:T(8,128)(2,1)}, u32[]{:S(2)}) copy-start(bf16[3,2,4,128,128]{4,3,2,1,0:T(8,128)(2,1)} %param.26) | copy-start | bytes 2359300
  6.5 128.6 %copy-start.4 = (bf16[3,2,4,128,128]{4,3,2,1,0:T(8,128)(2,1)S(1)}, bf16[3,2,4,128,128]{4,3,2,1,0:T(8,128)(2,1)}, u32[]{:S(2)}) copy-start(bf16[3,2,4,128,128]{4,3,2,1,0:T(8,128)(2,1)} %param.25) | copy-start | bytes 2359300
  6.5 65.8 %all-gather.16.cloned.1.call-start = ((), (), s32[]{:S(2)}) async-start(), calls=%async_computation.3 | async-start | bytes 3538944 | tf_op jit(solution)/shard_map/all_gather | solution.py:62
  7.3 125.9 %all-gather.18.cloned.1.call-start = ((), (), s32[]{:S(2)}) async-start(), calls=%async_computation.4 | async-start | bytes 3538944 | tf_op jit(solution)/shard_map/all_gather | solution.py:63
  8.0 255.6 %all-gather.20.cloned.1.call-start = ((), (), s32[]{:S(2)}) async-start(), calls=%async_computation.5 | async-start | bytes 3538944 | tf_op jit(solution)/shard_map/all_gather | solution.py:65
  8.7 275.5 %reduce-scatter.4.cloned.1.call-start = ((), (), s32[]{:S(2)}) async-start(), calls=%async_computation.6 | async-start | bytes 81920 | tf_op jit(solution)/shard_map/reduce_scatter | solution.py:135
  73.8 60.9 %collective-permute-start.1 = (bf16[2,2,512]{2,1,0:T(2,128)(2,1)S(1)}, bf16[2,2,512]{2,1,0:T(2,128)(2,1)S(1)}, u32[]{:S(2)}, u32[]{:S(2)}) collective-permute-start(bf16[2,2,512]{2,1,0:T(2,128)(2,1)S(1)} %get-tuple-element.783), channel_id=1, source_target_pairs={{4,0},{8,4},{12,8},{16,12},{20,16},{24,20},{28,24},{5,1},{9,5},{13... | collective-permute-start | bytes 12296 | tf_op jit(solution)/shard_map/ppermute | solution.py:19
  75.1 59.6 %collective-permute-start = (bf16[2,2,512]{2,1,0:T(2,128)(2,1)S(1)}, bf16[2,2,512]{2,1,0:T(2,128)(2,1)S(1)}, u32[]{:S(2)}, u32[]{:S(2)}) collective-permute-start(bf16[2,2,512]{2,1,0:T(2,128)(2,1)S(1)} %get-tuple-element.784), channel_id=1, source_target_pairs={{0,4},{4,8},{8,12},{12,16},{16,20},{20,24},{24,28},{1,5},{5,9},{9,... | collective-permute-start | bytes 12296 | tf_op jit(solution)/shard_map/ppermute | solution.py:18
  265.8 199.9 %reduce-scatter.6.cloned.1.call-start = ((), (), s32[]{:S(2)}) async-start(), calls=%async_computation.7 | async-start | bytes 81920 | tf_op jit(solution)/shard_map/reduce_scatter | solution.py:135
  291.4 8.0 %collective-permute-start.3 = (bf16[2,2,512]{2,1,0:T(2,128)(2,1)S(1)}, bf16[2,2,512]{2,1,0:T(2,128)(2,1)S(1)}, u32[]{:S(2)}, u32[]{:S(2)}) collective-permute-start(bf16[2,2,512]{2,1,0:T(2,128)(2,1)S(1)} %get-tuple-element.773), channel_id=1, source_target_pairs={{4,0},{8,4},{12,8},{16,12},{20,16},{24,20},{28,24},{5,1},{9,5},{13... | collective-permute-start | bytes 12296 | tf_op jit(solution)/shard_map/ppermute | solution.py:19
  292.7 6.7 %collective-permute-start.2 = (bf16[2,2,512]{2,1,0:T(2,128)(2,1)S(1)}, bf16[2,2,512]{2,1,0:T(2,128)(2,1)S(1)}, u32[]{:S(2)}, u32[]{:S(2)}) collective-permute-start(bf16[2,2,512]{2,1,0:T(2,128)(2,1)S(1)} %get-tuple-element.774), channel_id=1, source_target_pairs={{0,4},{4,8},{8,12},{12,16},{16,20},{20,24},{24,28},{1,5},{5,9},{9,... | collective-permute-start | bytes 12296 | tf_op jit(solution)/shard_map/ppermute | solution.py:18
  301.8 144.9 %copy-start = (bf16[3,512,1024]{2,1,0:T(8,128)(2,1)S(1)}, bf16[3,512,1024]{2,1,0:T(8,128)(2,1)}, u32[]{:S(2)}) copy-start(bf16[3,512,1024]{2,1,0:T(8,128)(2,1)} %all-gather.20.cloned.1.call-done) | copy-start | bytes 9437188
  370.9 110.8 %copy-start.2 = (f32[1,1,512]{2,1,0:T(1,128)S(1)}, f32[1,1,512]{2,1,0:T(1,128)}, u32[]{:S(2)}) copy-start(f32[1,1,512]{2,1,0:T(1,128)} %get-tuple-element.857) | copy-start | bytes 6148
  405.3 80.4 %copy-start.1 = (f32[1,1,512]{2,1,0:T(1,128)S(1)}, f32[1,1,512]{2,1,0:T(1,128)}, u32[]{:S(2)}) copy-start(f32[1,1,512]{2,1,0:T(1,128)} %get-tuple-element.841) | copy-start | bytes 6148
  447.7 203.4 %reduce-scatter.8.cloned.1.call-start = ((), (), s32[]{:S(2)}) async-start(), calls=%async_computation.8 | async-start | bytes 81920 | tf_op jit(solution)/shard_map/reduce_scatter | solution.py:135
  473.5 8.2 %collective-permute-start.5 = (bf16[2,2,512]{2,1,0:T(2,128)(2,1)S(1)}, bf16[2,2,512]{2,1,0:T(2,128)(2,1)S(1)}, u32[]{:S(2)}, u32[]{:S(2)}) collective-permute-start(bf16[2,2,512]{2,1,0:T(2,128)(2,1)S(1)} %get-tuple-element.763), channel_id=1, source_target_pairs={{4,0},{8,4},{12,8},{16,12},{20,16},{24,20},{28,24},{5,1},{9,5},{13... | collective-permute-start | bytes 12296 | tf_op jit(solution)/shard_map/ppermute | solution.py:19
  474.8 6.9 %collective-permute-start.4 = (bf16[2,2,512]{2,1,0:T(2,128)(2,1)S(1)}, bf16[2,2,512]{2,1,0:T(2,128)(2,1)S(1)}, u32[]{:S(2)}, u32[]{:S(2)}) collective-permute-start(bf16[2,2,512]{2,1,0:T(2,128)(2,1)S(1)} %get-tuple-element.764), channel_id=1, source_target_pairs={{0,4},{4,8},{8,12},{12,16},{16,20},{20,24},{24,28},{1,5},{5,9},{9,... | collective-permute-start | bytes 12296 | tf_op jit(solution)/shard_map/ppermute | solution.py:18
Sparse Core Ops, SparseCore 0:
  9.5 62.7 all-gather.15
  74.5 58.6 all-gather.17
  135.2 62.0 all-gather.19
  265.9 18.3 reduce-scatter.3
  447.8 17.8 reduce-scatter.5
  633.4 17.6 reduce-scatter.7
where the time goes:
time: 660 us; the launch traced here: 658 us
  blocking collectives  392 us (59%)
  waiting for transfers between devices  162 us (25%)
  other arithmetic  28.7 us (4%)
  matrix products  20.8 us (3%)
  local copies, waits for them, and re-layouts  19.3 us (3%)
  starting transfers between devices  17.9 us (3%)
  between operations  15.6 us (2%)
    all_gather x12, blocking collectives, carried_in(): pieces = jax.tree.map(lambda part: lax.all_gather(part, axis), value)  375 us
    all_gather x1, waiting for transfers between devices, body(): lax.all_gather(gate_weight, 'sp', axis=1, tiled=True)  53.5 us
    reduce_scatter x3, waiting for transfers between devices, body(): lax.psum_scatter(partial_terms.astype(jnp.bfloat16), 'tp', scatter_dimens...  53.5 us
    all_gather x1, waiting for transfers between devices, body(): lax.all_gather(in_weight, 'sp', axis=1, tiled=True)  53.2 us
    all_gather x3, blocking collectives, body(): gathered = lax.all_gather(state, 'tp', axis=2, tiled=True)  17.3 us
    ppermute x3, starting transfers between devices, extended(): before = lax.ppermute(last, axis, up)  13.8 us
  transfers between devices with their start and end apart: 12, of which 5 were waited for; matrix products, arithmetic and copies ran while one was open for 2% of the time, Pallas kernels for 0%

commit v1 on v0

--- a/solution.py
+++ b/solution.py
@@ -60,7 +60,7 @@
     chan_width = in_weight.shape[2]
     in_whole, gate_whole = (
         lax.all_gather(in_weight, "sp", axis=1, tiled=True),
-        lax.all_gather(gate_weight, "sp", axis=1, tiled=True),
+        jnp.concatenate(lax.all_gather(gate_weight, "sp"), axis=1),
     )
     out_whole = lax.all_gather(out_weight, "sp", axis=2, tiled=True)
     state = tokens

time: 660 us -> 636 us (0.964)
  other arithmetic: 28.7 us -> 6.14 us
  waiting for transfers between devices: 162 us -> 182 us
  local copies, waits for them, and re-layouts: 19.3 us -> 10.1 us
    ppermute x3, waiting for transfers between devices: 0.02 us -> 11.9 us  [extended(): after = lax.ppermute(initial, axis, down)]
    select_n x42, other arithmetic: 10.3 us -> 0.73 us  [hop(): jnp.where(position < mine, new, old)]
  transfers between devices with their start and end apart: 12 -> 12, of which waited for: 5 -> 8; matrix products, arithmetic and copies ran while one was open for 2% -> 2% of each run, Pallas kernels for 0% -> 0%
where the time goes in v1:
time: 636 us
  blocking collectives  386 us (61%)
  waiting for transfers between devices  182 us (29%)
  matrix products  20.9 us (3%)
  between operations  15.8 us (2%)
  starting transfers between devices  13.5 us (2%)
  local copies, waits for them, and re-layouts  10.1 us (2%)
    all_gather x12, blocking collectives, carried_in(): pieces = jax.tree.map(lambda part: lax.all_gather(part, axis), value)  369 us
    all_gather x1, waiting for transfers between devices, body(): lax.all_gather(in_weight, 'sp', axis=1, tiled=True)  58.8 us
    reduce_scatter x3, waiting for transfers between devices, body(): lax.psum_scatter(partial_terms.astype(jnp.bfloat16), 'tp', scatter_dimens...  55 us
    all_gather x1, waiting for transfers between devices, body(): lax.all_gather(gate_weight, 'sp')  54.4 us
    all_gather x3, blocking collectives, body(): gathered = lax.all_gather(state, 'tp', axis=2, tiled=True)  17.3 us
  transfers between devices with their start and end apart: 12, of which 8 were waited for; matrix products, arithmetic and copies ran while one was open for 2% of the time, Pallas kernels for 0%

profile of v1, /device:TPU:0, one launch (start us, length us, event | category | flops | bytes accessed | tf_op | source)
XLA Modules:
  0.0 635.6 jit_solution(15332917014940081037)
XLA Ops:
  8.8 6.5 %all_gather.57 = bf16[2,16,1024]{2,1,0:T(8,128)(2,1)S(1)} all-gather(bf16[2,16,256]{2,1,0:T(8,128)(2,1)} %param.21), channel_id=1, replica_groups=mesh['sp'=8,'tp'=4] {'tp'}, dimensions={2}, use_global_device_ids=true | all-gather | bytes 81920 | tf_op jit(solution)/shard_map/all_gather | solution.py:68
  17.9 54.4 %all-gather.21.cloned.1.call-done = bf16[24,128,512]{2,1,0:T(8,128)(2,1)} async-done(((bf16[3,128,512]{2,1,0:T(8,128)(2,1)}), bf16[24,128,512]{2,1,0:T(8,128)(2,1)}) %all-gather.21.cloned.1.call-update) | async-done | bytes 3145744 | tf_op jit(solution)/shard_map/all_gather | solution.py:63
  72.3 2.1 fusion.165
  74.4 58.8 %all-gather.17.cloned.1.call-done = bf16[3,1024,512]{2,1,0:T(8,128)(2,1)} async-done(((bf16[3,128,512]{2,1,0:T(8,128)(2,1)}), bf16[3,1024,512]{2,1,0:T(8,128)(2,1)}) %all-gather.17.cloned.1.call-update) | async-done | bytes 3145744 | tf_op jit(solution)/shard_map/all_gather | solution.py:62
  134.7 2.5 collective-permute-start
  138.8 4.3 collective-permute-done.1
  150.9 31.2 %all-gather.2 = f32[16,1,512]{2,1,0:T(1,128)S(1)} all-gather(f32[2,1,512]{2,1,0:T(1,128)S(1)} %slice_add_fusion.19), channel_id=4, replica_groups=mesh['sp'=8,'tp'=4] {'sp'}, dimensions={0}, use_global_device_ids=true | all-gather | bytes 36864 | tf_op jit(solution)/shard_map/all_gather | solution.py:26
  182.2 31.1 %all-gather.3 = f32[16,1,512]{2,1,0:T(1,128)S(1)} all-gather(f32[2,1,512]{2,1,0:T(1,128)S(1)} %slice_add_fusion.16), channel_id=5, replica_groups=mesh['sp'=8,'tp'=4] {'sp'}, dimensions={0}, use_global_device_ids=true | all-gather | bytes 36864 | tf_op jit(solution)/shard_map/all_gather | solution.py:26
  213.5 30.6 %all-gather = f32[16,1,512]{2,1,0:T(1,128)S(1)} all-gather(f32[2,1,512]{2,1,0:T(1,128)S(1)} %slice_add_fusion.23), channel_id=2, replica_groups=mesh['sp'=8,'tp'=4] {'sp'}, dimensions={0}, use_global_device_ids=true | all-gather | bytes 36864 | tf_op jit(solution)/shard_map/all_gather | solution.py:26
  244.2 30.6 %all-gather.1 = f32[16,1,512]{2,1,0:T(1,128)S(1)} all-gather(f32[2,1,512]{2,1,0:T(1,128)S(1)} %slice_add_fusion.20), channel_id=3, replica_groups=mesh['sp'=8,'tp'=4] {'sp'}, dimensions={0}, use_global_device_ids=true | all-gather | bytes 36864 | tf_op jit(solution)/shard_map/all_gather | solution.py:26
  275.6 2.1 convolution_convert_fusion.2
  277.8 19.3 %reduce-scatter.4.cloned.1.call-done = bf16[32,256]{1,0:T(8,128)(2,1)} async-done(((bf16[32,1024]{1,0:T(8,128)(2,1)}), bf16[32,256]{1,0:T(8,128)(2,1)}) %reduce-scatter.4.cloned.1.call-update) | async-done | bytes 16400 | tf_op jit(solution)/shard_map/reduce_scatter | solution.py:135
  297.1 5.4 all_gather.66
  302.8 1.5 convolution_convert_fusion.6
  304.3 3.4 collective-permute-start.2
  309.3 3.9 collective-permute-done.3
  319.2 30.7 %all-gather.7 = f32[16,1,512]{2,1,0:T(1,128)S(1)} all-gather(f32[2,1,512]{2,1,0:T(1,128)S(1)} %slice_add_fusion.11), channel_id=9, replica_groups=mesh['sp'=8,'tp'=4] {'sp'}, dimensions={0}, use_global_device_ids=true | all-gather | bytes 36864 | tf_op jit(solution)/shard_map/all_gather | solution.py:26
  350.0 30.6 %all-gather.8 = f32[16,1,512]{2,1,0:T(1,128)S(1)} all-gather(f32[2,1,512]{2,1,0:T(1,128)S(1)} %slice_add_fusion.8), channel_id=10, replica_groups=mesh['sp'=8,'tp'=4] {'sp'}, dimensions={0}, use_global_device_ids=true | all-gather | bytes 36864 | tf_op jit(solution)/shard_map/all_gather | solution.py:26
  381.1 30.6 %all-gather.5 = f32[16,1,512]{2,1,0:T(1,128)S(1)} all-gather(f32[2,1,512]{2,1,0:T(1,128)S(1)} %slice_add_fusion.15), channel_id=7, replica_groups=mesh['sp'=8,'tp'=4] {'sp'}, dimensions={0}, use_global_device_ids=true | all-gather | bytes 36864 | tf_op jit(solution)/shard_map/all_gather | solution.py:26
  411.8 30.6 %all-gather.6 = f32[16,1,512]{2,1,0:T(1,128)S(1)} all-gather(f32[2,1,512]{2,1,0:T(1,128)S(1)} %slice_add_fusion.12), channel_id=8, replica_groups=mesh['sp'=8,'tp'=4] {'sp'}, dimensions={0}, use_global_device_ids=true | all-gather | bytes 36864 | tf_op jit(solution)/shard_map/all_gather | solution.py:26
  442.9 2.1 convolution_convert_fusion.1
  445.1 17.8 %reduce-scatter.6.cloned.1.call-done = bf16[32,256]{1,0:T(8,128)(2,1)} async-done(((bf16[32,1024]{1,0:T(8,128)(2,1)}), bf16[32,256]{1,0:T(8,128)(2,1)}) %reduce-scatter.6.cloned.1.call-update) | async-done | bytes 16400 | tf_op jit(solution)/shard_map/reduce_scatter | solution.py:135
  463.0 5.4 all_gather.71
  468.6 1.5 convolution_convert_fusion.4
  470.1 3.4 collective-permute-start.4
  475.3 3.7 collective-permute-done.5
  485.0 30.7 %all-gather.11 = f32[16,1,512]{2,1,0:T(1,128)S(1)} all-gather(f32[2,1,512]{2,1,0:T(1,128)S(1)} %slice_add_fusion.3), channel_id=13, replica_groups=mesh['sp'=8,'tp'=4] {'sp'}, dimensions={0}, use_global_device_ids=true | all-gather | bytes 36864 | tf_op jit(solution)/shard_map/all_gather | solution.py:26
  515.8 30.6 %all-gather.12 = f32[16,1,512]{2,1,0:T(1,128)S(1)} all-gather(f32[2,1,512]{2,1,0:T(1,128)S(1)} %slice_add_fusion), channel_id=14, replica_groups=mesh['sp'=8,'tp'=4] {'sp'}, dimensions={0}, use_global_device_ids=true | all-gather | bytes 36864 | tf_op jit(solution)/shard_map/all_gather | solution.py:26
  546.9 30.6 %all-gather.9 = f32[16,1,512]{2,1,0:T(1,128)S(1)} all-gather(f32[2,1,512]{2,1,0:T(1,128)S(1)} %slice_add_fusion.7), channel_id=11, replica_groups=mesh['sp'=8,'tp'=4] {'sp'}, dimensions={0}, use_global_device_ids=true | all-gather | bytes 36864 | tf_op jit(solution)/shard_map/all_gather | solution.py:26
  577.6 30.6 %all-gather.10 = f32[16,1,512]{2,1,0:T(1,128)S(1)} all-gather(f32[2,1,512]{2,1,0:T(1,128)S(1)} %slice_add_fusion.4), channel_id=12, replica_groups=mesh['sp'=8,'tp'=4] {'sp'}, dimensions={0}, use_global_device_ids=true | all-gather | bytes 36864 | tf_op jit(solution)/shard_map/all_gather | solution.py:26
  608.7 2.1 convolution_convert_fusion
  610.8 17.9 %reduce-scatter.8.cloned.1.call-done = bf16[32,256]{1,0:T(8,128)(2,1)} async-done(((bf16[32,1024]{1,0:T(8,128)(2,1)}), bf16[32,256]{1,0:T(8,128)(2,1)}) %reduce-scatter.8.cloned.1.call-update) | async-done | bytes 16400 | tf_op jit(solution)/shard_map/reduce_scatter | solution.py:135
  (497 shorter events, 33.8 us)
Async XLA Ops:
  6.5 65.7 %all-gather.21.cloned.1.call-start = ((), (), s32[]{:S(2)}) async-start(), calls=%async_computation.8 | async-start | bytes 3538944 | tf_op jit(solution)/shard_map/all_gather | solution.py:63
  7.3 125.9 %all-gather.17.cloned.1.call-start = ((), (), s32[]{:S(2)}) async-start(), calls=%async_computation.3 | async-start | bytes 3538944 | tf_op jit(solution)/shard_map/all_gather | solution.py:62
  8.0 267.6 %all-gather.19.cloned.1.call-start = ((), (), s32[]{:S(2)}) async-start(), calls=%async_computation.4 | async-start | bytes 3538944 | tf_op jit(solution)/shard_map/all_gather | solution.py:65
  8.7 288.4 %reduce-scatter.4.cloned.1.call-start = ((), (), s32[]{:S(2)}) async-start(), calls=%async_computation.5 | async-start | bytes 81920 | tf_op jit(solution)/shard_map/reduce_scatter | solution.py:135
  134.7 4.0 collective-permute-start
  137.2 5.9 collective-permute-start.1
  182.2 131.0 %copy-start = (bf16[3,2,4,128,128]{4,3,2,1,0:T(8,128)(2,1)S(1)}, bf16[3,2,4,128,128]{4,3,2,1,0:T(8,128)(2,1)}, u32[]{:S(2)}) copy-start(bf16[3,2,4,128,128]{4,3,2,1,0:T(8,128)(2,1)} %param.25) | copy-start | bytes 2359300
  277.8 185.2 %reduce-scatter.6.cloned.1.call-start = ((), (), s32[]{:S(2)}) async-start(), calls=%async_computation.6 | async-start | bytes 81920 | tf_op jit(solution)/shard_map/reduce_scatter | solution.py:135
  304.3 5.0 collective-permute-start.2
  307.7 5.5 collective-permute-start.3
  445.0 183.7 %reduce-scatter.8.cloned.1.call-start = ((), (), s32[]{:S(2)}) async-start(), calls=%async_computation.7 | async-start | bytes 81920 | tf_op jit(solution)/shard_map/reduce_scatter | solution.py:135
  470.1 5.1 collective-permute-start.4
  473.5 5.5 collective-permute-start.5
Sparse Core Ops, SparseCore 0:
  9.5 62.7 all-gather.20
  74.5 58.6 all-gather.16
  135.2 61.8 all-gather.18
  277.9 19.2 reduce-scatter.3
  445.2 17.7 reduce-scatter.5
  611.0 17.7 reduce-scatter.7
